TPU v7x, 512 devices: a whole 4x4x16 slice. The times are simulated.
512 devices in a mesh: fs: 32 (over z, core), tp: 16 (over y, x).
Axes of the slice: x: 4, y: 4, z: 16, core: 2. Of those that a mesh axis runs over, the one named last changes fastest.
Arguments:
- late_input: bfloat16 [4096, 2048], P('fs'), may hold values from -6 to 6
- early_input: bfloat16 [4096, 2048], P('fs'), may hold values from -6 to 6
- early_mid: bfloat16 [4096, 2048], P('fs'), may hold values from -6 to 6
- cotangent: bfloat16 [4096, 2048], P('fs'), may hold values from -6 to 6
- gain_first: float32 [2048], replicated, may hold values from 0.1 to 1.9
- gain_second: float32 [2048], replicated, may hold values from 0.1 to 1.9
- gate_first: bfloat16 [2048, 2816], P('fs', 'tp'), may hold values from -0.125 to 0.125
- up_first: bfloat16 [2048, 2816], P('fs', 'tp'), may hold values from -0.125 to 0.125
- down_first: bfloat16 [2816, 2048], P('tp', 'fs'), may hold values from -0.109375 to 0.109375
- gate_second: bfloat16 [2048, 2816], P('fs', 'tp'), may hold values from -0.125 to 0.125
- up_second: bfloat16 [2048, 2816], P('fs', 'tp'), may hold values from -0.125 to 0.125
- down_second: bfloat16 [2816, 2048], P('tp', 'fs'), may hold values from -0.109375 to 0.109375
- sum_gate_first: float32 [2048, 2816], P('fs', 'tp'), may hold values from -256 to 256
- sum_up_first: float32 [2048, 2816], P('fs', 'tp'), may hold values from -256 to 256
- sum_down_first: float32 [2816, 2048], P('tp', 'fs'), may hold values from -256 to 256
- sum_gate_second: float32 [2048, 2816], P('fs', 'tp'), may hold values from -256 to 256
- sum_up_second: float32 [2048, 2816], P('fs', 'tp'), may hold values from -256 to 256
- sum_down_second: float32 [2816, 2048], P('tp', 'fs'), may hold values from -256 to 256
Outputs:
- late_mid: bfloat16 [4096, 2048], P('fs')
- late_out: bfloat16 [4096, 2048], P('fs')
- input_grad: bfloat16 [4096, 2048], P('fs')
- new_gate_first: float32 [2048, 2816], P('fs', 'tp')
- new_up_first: float32 [2048, 2816], P('fs', 'tp')
- new_down_first: float32 [2816, 2048], P('tp', 'fs')
- new_gate_second: float32 [2048, 2816], P('fs', 'tp')
- new_up_second: float32 [2048, 2816], P('fs', 'tp')
- new_down_second: float32 [2816, 2048], P('tp', 'fs')
All inputs are finite; a program needn't handle non-finite values.
Results may differ from a plain program's by a relative error of at most 0.015.
Values may be sent and summed in bfloat16 or wider, within the bound.
No kernel may reach another device: no remote copies, remote signals or barrier semaphores. Data moves between devices by JAX's collectives and lax.ppermute only.
A program may use at most 128 MiB of HBM per device.

v0:
```python
import jax
import jax.numpy as jnp
from jax import lax
from jax.sharding import PartitionSpec as P

norm_eps = 1e-06


def sent_together(arrays, axis, dim, along):
    both = jnp.concatenate(arrays, axis=along)
    whole, at, outs = (lax.all_gather(both, axis, axis=dim, tiled=True), 0, [])
    for a in arrays:
        outs.append(lax.slice_in_dim(whole, at, at + a.shape[along], axis=along))
        at += a.shape[along]
    return tuple(outs)


def gather_turned(arrays, axis, dims):
    turned = [jnp.moveaxis(a, dim, 0) for a, dim in zip(arrays, dims)]
    widths = [t[0].size for t in turned]
    both = jnp.concatenate([t.reshape(-1, w) for t, w in zip(turned, widths)], axis=1)
    whole = lax.all_gather(both, axis, axis=0, tiled=True)
    blocks = jnp.split(whole, [sum(widths[:k]) for k in range(1, len(widths))], axis=1)
    return tuple(
        (
            jnp.moveaxis(b.reshape(-1, *t.shape[1:]), 0, dim)
            for b, t, dim in zip(blocks, turned, dims)
        )
    )


def normalize(values, gain_vector):
    widened = values.astype(jnp.float32)
    factor = lax.rsqrt(jnp.mean(widened * widened, axis=-1, keepdims=True) + norm_eps)
    normed = (widened * factor * gain_vector).astype(jnp.bfloat16)
    return (widened, factor, normed)


def block_forward(values, params):
    gain_vector, w_gate, w_up, w_down = params
    widened, factor, normed = normalize(values, gain_vector)
    gate_pre = jnp.dot(normed, w_gate, preferred_element_type=jnp.float32)
    up_pre = jnp.dot(normed, w_up, preferred_element_type=jnp.float32)
    hidden = (jax.nn.silu(gate_pre) * up_pre).astype(jnp.bfloat16)
    branch = lax.psum(
        jnp.dot(hidden, w_down, preferred_element_type=jnp.float32).astype(jnp.bfloat16), "tp"
    ).astype(jnp.float32)
    return (widened + 0.5 * branch).astype(jnp.bfloat16)


def block_backward(values, cotangent, params):
    gain_vector, w_gate, w_up, w_down = params
    widened, factor, normed = normalize(values, gain_vector)
    gate_pre = jnp.dot(normed, w_gate, preferred_element_type=jnp.float32)
    up_pre = jnp.dot(normed, w_up, preferred_element_type=jnp.float32)
    sigmoid_gate = jax.nn.sigmoid(gate_pre)
    activated = gate_pre * sigmoid_gate
    hidden = (activated * up_pre).astype(jnp.bfloat16)
    hidden_grad = 0.5 * jnp.einsum(
        "td,fd->tf", cotangent, w_down, preferred_element_type=jnp.float32
    )
    gate_grad = (
        hidden_grad * up_pre * sigmoid_gate * (1.0 + gate_pre * (1.0 - sigmoid_gate))
    ).astype(jnp.bfloat16)
    up_grad = (hidden_grad * activated).astype(jnp.bfloat16)
    partial_value = jnp.einsum("tf,df->td", gate_grad, w_gate, preferred_element_type=jnp.float32)
    partial_value = partial_value + jnp.einsum(
        "tf,df->td", up_grad, w_up, preferred_element_type=jnp.float32
    )
    normed_grad = lax.psum(partial_value.astype(jnp.bfloat16), "tp").astype(jnp.float32)
    scaled = normed_grad * gain_vector
    unit_rows = widened * factor
    rows_grad = cotangent.astype(jnp.float32) + factor * (
        scaled - unit_rows * jnp.mean(scaled * unit_rows, axis=-1, keepdims=True)
    )
    return (rows_grad, (normed, cotangent, gate_grad, up_grad, hidden))


def fold_pair(pieces, columns_in):
    return (
        jnp.einsum("td,tf->df", columns_in, pieces[0], preferred_element_type=jnp.float32),
        jnp.einsum("td,tf->df", columns_in, pieces[1], preferred_element_type=jnp.float32),
    )


def fold_block(pieces, columns_in, columns_out):
    paired = fold_pair(pieces[0:2], columns_in)
    return paired + (
        jnp.einsum("tf,td->fd", pieces[2], columns_out, preferred_element_type=jnp.float32),
    )


def per_device(
    late_input,
    early_input,
    early_mid,
    cotangent,
    gain_first,
    gain_second,
    gate_first,
    up_first,
    down_first,
    gate_second,
    up_second,
    down_second,
    sum_gate_first,
    sum_up_first,
    sum_down_first,
    sum_gate_second,
    sum_up_second,
    sum_down_second,
):
    rows_in = sent_together((gate_first, up_first, gate_second, up_second), "fs", 0, 1)
    cols_out = gather_turned((down_first, down_second), "fs", (1, 1))
    first_params = (gain_first, rows_in[0], rows_in[1], cols_out[0])
    second_params = (gain_second, rows_in[2], rows_in[3], cols_out[1])
    late_mid = block_forward(late_input, first_params)
    late_out = block_forward(late_mid, second_params)
    mid_grad, saved_second = block_backward(early_mid, cotangent, second_params)
    mid_grad = mid_grad.astype(jnp.bfloat16)
    rows_grad, saved_first = block_backward(early_input, mid_grad, first_params)
    pieces = sent_together(
        (
            saved_second[2],
            saved_second[3],
            saved_second[4],
            saved_first[2],
            saved_first[3],
            saved_first[4],
        ),
        "fs",
        0,
        1,
    )
    upper = fold_block(
        pieces[0:3],
        lax.all_to_all(saved_second[0], "fs", split_axis=1, concat_axis=0, tiled=True),
        lax.all_to_all(saved_second[1], "fs", split_axis=1, concat_axis=0, tiled=True),
    )
    lower = fold_block(
        pieces[3:6],
        lax.all_to_all(saved_first[0], "fs", split_axis=1, concat_axis=0, tiled=True),
        lax.all_to_all(saved_first[1], "fs", split_axis=1, concat_axis=0, tiled=True),
    )
    result = upper + lower
    grads_second = (result[0], result[1], 0.5 * result[2])
    grads_first = (result[3], result[4], 0.5 * result[5])
    return (
        late_mid,
        late_out,
        rows_grad.astype(jnp.bfloat16),
        sum_gate_first + grads_first[0],
        sum_up_first + grads_first[1],
        sum_down_first + grads_first[2],
        sum_gate_second + grads_second[0],
        sum_up_second + grads_second[1],
        sum_down_second + grads_second[2],
    )


def solution(mesh):
    in_specs = (
        P("fs", None),
        P("fs", None),
        P("fs", None),
        P("fs", None),
        P(),
        P(),
        P("fs", "tp"),
        P("fs", "tp"),
        P("tp", "fs"),
        P("fs", "tp"),
        P("fs", "tp"),
        P("tp", "fs"),
        P("fs", "tp"),
        P("fs", "tp"),
        P("tp", "fs"),
        P("fs", "tp"),
        P("fs", "tp"),
        P("tp", "fs"),
    )
    out_specs = (
        P("fs", None),
        P("fs", None),
        P("fs", None),
        P("fs", "tp"),
        P("fs", "tp"),
        P("tp", "fs"),
        P("fs", "tp"),
        P("fs", "tp"),
        P("tp", "fs"),
    )
    return jax.shard_map(
        per_device, mesh=mesh, in_specs=in_specs, out_specs=out_specs, check_vma=False
    )
```

profile of v0, /device:TPU:1, one launch (start us, length us, event | category | flops | bytes accessed | tf_op | source)
XLA Modules:
  0.0 560.9 jit_solution(5887314163387625684)
XLA Ops:
  7.2 0.0 all-gather.6.cloned.1.call-start
  7.2 1.5 pad_maximum_fusion.1
  8.7 0.0 all-gather.6.cloned.1.call-update
  8.7 0.0 all-gather.4.cloned.1.call-start
  8.8 1.6 pad_maximum_fusion
  10.3 0.0 all-gather.4.cloned.1.call-update
  10.4 0.0 all-reduce.7.cloned.1.call-start
  10.4 1.2 fusion.61
  11.6 1.2 fusion.53
  12.9 1.2 fusion.60
  14.1 2.0 fusion.47
  16.1 71.3 %all-gather.6.cloned.1.call-done = bf16[2048,352]{1,0:T(8,128)(2,1)} async-done(((bf16[64,352]{1,0:T(8,128)(2,1)}), bf16[2048,352]{1,0:T(8,128)(2,1)}) %all-gather.6.cloned.1.call-update) | async-done | bytes 1441808 | tf_op jit(solution)/shard_map/all_gather | solution.py:22
  87.5 2.1 fusion.20
  89.6 70.4 %all-gather.4.cloned.1.call-done = bf16[2048,704]{1,0:T(8,128)(2,1)} async-done(((bf16[64,704]{1,0:T(8,128)(2,1)}), bf16[2048,704]{1,0:T(8,128)(2,1)}) %all-gather.4.cloned.1.call-update) | async-done | bytes 2883600 | tf_op jit(solution)/shard_map/all_gather | solution.py:11
  160.0 2.6 fusion.74
  162.6 3.2 constant_dynamic-update-slice_fusion.3
  165.8 0.6 constant_dynamic-update-slice_fusion.2
  166.5 1.6 fusion.93
  168.1 3.9 convolution_convert_fusion.1
  172.0 0.7 fusion.78
  172.6 1.5 fusion
  174.1 0.0 all-reduce.7.cloned.1.call-update
  174.1 0.2 all-reduce.5.cloned.1.call-start
  174.4 1.2 fusion.54
  175.6 0.8 fusion.125
  176.4 0.1 copy-done.5
  176.5 1.0 fusion.85
  177.5 110.1 %all-reduce.7.cloned.1.call-done = (bf16[128,2048]{1,0:T(8,128)(2,1)}, bf16[128,2048]{1,0:T(8,128)(2,1)}) async-done(((bf16[128,2048]{1,0:T(8,128)(2,1)}, bf16[128,2048]{1,0:T(8,128)(2,1)}), (bf16[128,2048]{1,0:T(8,128)(2,1)}, bf16[128,2048]{1,0:T(8,128)(2,1)})) %all-reduce.7.cloned.1.call-update) | async-done | bytes 1048592 | tf_op jit(solution)/shard_map/psum | solution.py:45
  287.6 1.7 fusion.65
  289.3 1.7 fusion.48
  291.0 1.8 fusion.52
  292.8 0.8 copy-done.2
  293.6 0.5 convolution_multiply_fusion
  294.1 1.1 constant_dynamic-update-slice_fusion.1
  295.2 0.7 constant_dynamic-update-slice_fusion
  295.9 1.7 fusion.82
  297.6 4.0 convolution_convert_fusion
  301.6 0.5 fusion.89
  302.1 1.5 fusion.1
  303.5 0.0 all-reduce.5.cloned.1.call-update
  303.6 0.0 all-gather.8.cloned.1.call-start
  303.6 0.7 fusion.126
  304.3 0.0 all-gather.8.cloned.1.call-update
  304.3 2.1 copy.27
  306.4 14.7 %all-to-all-start = ((bf16[128,32,64]{0,2,1:T(8,128)(2,1)}), bf16[128,32,64]{0,2,1:T(8,128)(2,1)S(1)}, u32[]{:S(2)}, u32[]{:S(2)}) async-start(bf16[128,32,64]{0,2,1:T(8,128)(2,1)} %bitcast.3), calls=%async_computation | async-start | bytes 1048576 | tf_op jit(solution)/shard_map/all_to_all | solution.py:142
  321.1 1.0 copy.31
  322.2 32.5 %all-to-all-done = bf16[128,32,64]{0,2,1:T(8,128)(2,1)S(1)} async-done(((bf16[128,32,64]{0,2,1:T(8,128)(2,1)}), bf16[128,32,64]{0,2,1:T(8,128)(2,1)S(1)}, u32[]{:S(2)}, u32[]{:S(2)}) %all-to-all-start) | async-done | bytes 524320 | tf_op jit(solution)/shard_map/all_to_all | solution.py:142
  354.6 4.2 all-to-all-start.2
  358.8 1.0 copy.29
  359.8 32.5 %all-to-all-done.2 = bf16[128,32,64]{0,2,1:T(8,128)(2,1)S(1)} async-done(((bf16[128,32,64]{0,2,1:T(8,128)(2,1)}), bf16[128,32,64]{0,2,1:T(8,128)(2,1)S(1)}, u32[]{:S(2)}, u32[]{:S(2)}) %all-to-all-start.2) | async-done | bytes 524320 | tf_op jit(solution)/shard_map/all_to_all | solution.py:137
  392.3 5.0 all-to-all-start.1
  397.4 1.0 copy.33
  398.4 22.9 %all-reduce.5.cloned.1.call-done = (bf16[128,2048]{1,0:T(8,128)(2,1)}, bf16[128,2048]{1,0:T(8,128)(2,1)}) async-done(((bf16[128,2048]{1,0:T(8,128)(2,1)}, bf16[128,2048]{1,0:T(8,128)(2,1)}), (bf16[128,2048]{1,0:T(8,128)(2,1)}, bf16[128,2048]{1,0:T(8,128)(2,1)})) %all-reduce.5.cloned.1.call-update) | async-done | bytes 1048592 | tf_op jit(solution)/shard_map/psum | solution.py:45
  421.2 1.4 fusion.55
  422.6 8.3 %all-to-all-done.1 = bf16[128,32,64]{0,2,1:T(8,128)(2,1)} async-done(((bf16[128,32,64]{0,2,1:T(8,128)(2,1)}), bf16[128,32,64]{0,2,1:T(8,128)(2,1)}, u32[]{:S(2)}, u32[]{:S(2)}) %all-to-all-start.1) | async-done | bytes 524320 | tf_op jit(solution)/shard_map/all_to_all | solution.py:143
  430.9 6.1 %all-to-all-start.3 = ((bf16[128,32,64]{0,2,1:T(8,128)(2,1)}), bf16[128,32,64]{0,2,1:T(8,128)(2,1)S(1)}, u32[]{:S(2)}, u32[]{:S(2)}) async-start(bf16[128,32,64]{0,2,1:T(8,128)(2,1)} %bitcast.9), calls=%async_computation.3 | async-start | bytes 1048576 | tf_op jit(solution)/shard_map/all_to_all | solution.py:138
  437.1 2.7 fusion.59
  439.8 98.8 %all-gather.8.cloned.1.call-done = bf16[4096,1056]{0,1:T(8,128)(2,1)} async-done(((bf16[128,1056]{0,1:T(8,128)(2,1)}), bf16[4096,1056]{0,1:T(8,128)(2,1)}) %all-gather.8.cloned.1.call-update) | async-done | bytes 8650768 | tf_op jit(solution)/shard_map/all_gather | solution.py:11
  538.7 2.6 fusion.23
  541.2 2.6 fusion.26
  543.9 2.6 fusion.35
  546.4 2.6 fusion.38
  549.1 2.7 fusion.32
  551.8 2.6 fusion.44
  (43 shorter events, 0.1 us)
Async XLA Ops:
  7.2 80.3 %all-gather.6.cloned.1.call-start = ((), (), s32[]{:S(2)}) async-start(), calls=%async_computation.5 | async-start | bytes 1622016 | tf_op jit(solution)/shard_map/all_gather | solution.py:22
  8.7 151.3 %all-gather.4.cloned.1.call-start = ((), (), s32[]{:S(2)}) async-start(), calls=%async_computation.4 | async-start | bytes 3244032 | tf_op jit(solution)/shard_map/all_gather | solution.py:11
  10.4 277.2 %all-reduce.7.cloned.1.call-start = ((), (), s32[]{:S(2)}) async-start(), calls=%async_computation.8 | async-start | bytes 2097152 | tf_op jit(solution)/shard_map/psum | solution.py:45
  16.1 150.4 %copy-start.12 = (f32[2048]{0:T(1024)S(1)}, f32[2048]{0:T(1024)}, u32[]{:S(2)}) copy-start(f32[2048]{0:T(1024)} %param.22) | copy-start | bytes 24580
  160.0 6.5 %copy-start = (bf16[2048,704]{1,0:T(8,128)(2,1)S(1)}, bf16[2048,704]{1,0:T(8,128)(2,1)}, u32[]{:S(2)}) copy-start(bf16[2048,704]{1,0:T(8,128)(2,1)} %all-gather.4.cloned.1.call-done) | copy-start | bytes 8650756
  174.1 115.2 %copy-start.11 = (f32[2048]{0:T(1024)S(1)}, f32[2048]{0:T(1024)}, u32[]{:S(2)}) copy-start(f32[2048]{0:T(1024)} %param.23) | copy-start | bytes 24580
  174.1 247.1 %all-reduce.5.cloned.1.call-start = ((), (), s32[]{:S(2)}) async-start(), calls=%async_computation.7 | async-start | bytes 2097152 | tf_op jit(solution)/shard_map/psum | solution.py:45
  175.6 0.9 copy-start.5
  287.6 6.0 %copy-start.10 = (bf16[2048,352]{1,0:T(8,128)(2,1)S(1)}, bf16[2048,352]{1,0:T(8,128)(2,1)}, u32[]{:S(2)}) copy-start(bf16[2048,352]{1,0:T(8,128)(2,1)} %all-gather.6.cloned.1.call-done) | copy-start | bytes 4325380
  287.6 6.5 %copy-start.6 = (bf16[128,2048]{1,0:T(8,128)(2,1)S(1)}, bf16[128,2048]{1,0:T(8,128)(2,1)}, u32[]{:S(2)}) copy-start(bf16[128,2048]{1,0:T(8,128)(2,1)} %copy-done.5) | copy-start | bytes 1572868
  289.2 6.6 %copy-start.8 = (bf16[128,2048]{1,0:T(8,128)(2,1)}, bf16[128,2048]{1,0:T(8,128)(2,1)S(1)}, u32[]{:S(2)}) copy-start(bf16[128,2048]{1,0:T(8,128)(2,1)S(1)} %get-tuple-element.22) | copy-start | bytes 1572868
  292.8 0.8 copy-start.2
  303.5 17.6 %copy-start.4 = (bf16[128,2048]{1,0:T(8,128)(2,1)S(1)}, bf16[128,2048]{1,0:T(8,128)(2,1)}, u32[]{:S(2)}) copy-start(bf16[128,2048]{1,0:T(8,128)(2,1)} %fusion.47) | copy-start | bytes 1572868
  303.5 55.3 %copy-start.3 = (bf16[128,2048]{1,0:T(8,128)(2,1)S(1)}, bf16[128,2048]{1,0:T(8,128)(2,1)}, u32[]{:S(2)}) copy-start(bf16[128,2048]{1,0:T(8,128)(2,1)} %copy-done.2) | copy-start | bytes 1572868
  303.6 235.1 %all-gather.8.cloned.1.call-start = ((), (), s32[]{:S(2)}) async-start(), calls=%async_computation.6 | async-start | bytes 8921088 | tf_op jit(solution)/shard_map/all_gather | solution.py:11
  304.3 93.1 %copy-start.7 = (bf16[128,2048]{1,0:T(8,128)(2,1)S(1)}, bf16[128,2048]{1,0:T(8,128)(2,1)}, u32[]{:S(2)}) copy-start(bf16[128,2048]{1,0:T(8,128)(2,1)} %param.21) | copy-start | bytes 1572868
  306.4 114.8 %copy-start.1 = (bf16[128,2048]{1,0:T(8,128)(2,1)S(1)}, bf16[128,2048]{1,0:T(8,128)(2,1)}, u32[]{:S(2)}) copy-start(bf16[128,2048]{1,0:T(8,128)(2,1)} %param.19) | copy-start | bytes 1572868
  306.4 48.2 %all-to-all-start = ((bf16[128,32,64]{0,2,1:T(8,128)(2,1)}), bf16[128,32,64]{0,2,1:T(8,128)(2,1)S(1)}, u32[]{:S(2)}, u32[]{:S(2)}) async-start(bf16[128,32,64]{0,2,1:T(8,128)(2,1)} %bitcast.3), calls=%async_computation | async-start | bytes 1048576 | tf_op jit(solution)/shard_map/all_to_all | solution.py:142
  354.6 82.4 %copy-start.9 = (bf16[128,2048]{1,0:T(8,128)(2,1)S(1)}, bf16[128,2048]{1,0:T(8,128)(2,1)}, u32[]{:S(2)}) copy-start(bf16[128,2048]{1,0:T(8,128)(2,1)} %copy-done.8) | copy-start | bytes 1572868
  354.6 37.7 %all-to-all-start.2 = ((bf16[128,32,64]{0,2,1:T(8,128)(2,1)}), bf16[128,32,64]{0,2,1:T(8,128)(2,1)S(1)}, u32[]{:S(2)}, u32[]{:S(2)}) async-start(bf16[128,32,64]{0,2,1:T(8,128)(2,1)} %bitcast.7), calls=%async_computation.2 | async-start | bytes 1048576 | tf_op jit(solution)/shard_map/all_to_all | solution.py:137
  392.3 38.6 %all-to-all-start.1 = ((bf16[128,32,64]{0,2,1:T(8,128)(2,1)}), bf16[128,32,64]{0,2,1:T(8,128)(2,1)}, u32[]{:S(2)}, u32[]{:S(2)}) async-start(bf16[128,32,64]{0,2,1:T(8,128)(2,1)} %bitcast.5), calls=%async_computation.1 | async-start | bytes 1048576 | tf_op jit(solution)/shard_map/all_to_all | solution.py:143
  398.4 140.3 %copy-start.13 = (f32[64,176]{1,0:T(8,128)S(1)}, f32[64,176]{1,0:T(8,128)}, u32[]{:S(2)}) copy-start(f32[64,176]{1,0:T(8,128)} %param.30) | copy-start | bytes 135172
  430.9 120.8 %all-to-all-start.3 = ((bf16[128,32,64]{0,2,1:T(8,128)(2,1)}), bf16[128,32,64]{0,2,1:T(8,128)(2,1)S(1)}, u32[]{:S(2)}, u32[]{:S(2)}) async-start(bf16[128,32,64]{0,2,1:T(8,128)(2,1)} %bitcast.9), calls=%async_computation.3 | async-start | bytes 1048576 | tf_op jit(solution)/shard_map/all_to_all | solution.py:138
  437.0 104.2 %copy-start.14 = (f32[64,176]{1,0:T(8,128)S(1)}, f32[64,176]{1,0:T(8,128)}, u32[]{:S(2)}) copy-start(f32[64,176]{1,0:T(8,128)} %param.31) | copy-start | bytes 135172
  439.8 104.0 %copy-start.15 = (f32[64,176]{1,0:T(8,128)S(1)}, f32[64,176]{1,0:T(8,128)}, u32[]{:S(2)}) copy-start(f32[64,176]{1,0:T(8,128)} %param.33) | copy-start | bytes 135172
  439.8 106.6 %copy-start.16 = (f32[64,176]{1,0:T(8,128)S(1)}, f32[64,176]{1,0:T(8,128)}, u32[]{:S(2)}) copy-start(f32[64,176]{1,0:T(8,128)} %param.34) | copy-start | bytes 135172
  541.2 7.8 %copy-start.17 = (f32[176,64]{0,1:T(8,128)S(1)}, f32[176,64]{0,1:T(8,128)}, u32[]{:S(2)}) copy-start(f32[176,64]{0,1:T(8,128)} %param.32) | copy-start | bytes 135172
  546.4 5.3 copy-start.18
Sparse Core Ops, SparseCore 0:
  10.7 76.7 all-gather.5
  90.1 69.8 all-gather.3
  174.2 113.2 all-reduce.6
  303.7 117.5 all-reduce.4
  423.1 115.4 all-gather.7
where the time goes:
time: 562 us; the launch traced here: 561 us
  waiting for transfers between devices  447 us (80%)
  matrix products  41.5 us (7%)
  starting transfers between devices  30.4 us (5%)
  other arithmetic  22 us (4%)
  between operations  14 us (2%)
  local copies, waits for them, and re-layouts  6.1 us (1%)
    all_gather x2, waiting for transfers between devices, sent_together(): whole, at, outs = (lax.all_gather(both, axis, axis=dim, tiled=True), 0, [])  169 us
    psum x2, waiting for transfers between devices, block_forward(): lax.psum(jnp.dot(hidden, w_down, preferred_element_type=jnp.float32).asty...  133 us
    all_gather x1, waiting for transfers between devices, gather_turned(): whole = lax.all_gather(both, axis, axis=0, tiled=True)  71.3 us
    all_to_all x1, waiting for transfers between devices, per_device(): lax.all_to_all(saved_second[0], 'fs', split_axis=1, concat_axis=0, tiled=...  32.5 us
    all_to_all x1, waiting for transfers between devices, per_device(): lax.all_to_all(saved_first[0], 'fs', split_axis=1, concat_axis=0, tiled=T...  32.5 us
    all_to_all x1, starting transfers between devices, per_device(): lax.all_to_all(saved_first[0], 'fs', split_axis=1, concat_axis=0, tiled=T...  14.7 us
  transfers between devices with their start and end apart: 9, of which 8 were waited for; matrix products, arithmetic and copies ran while one was open for 6% of the time, Pallas kernels for 0%

commit v1 on v0

--- a/solution.py
+++ b/solution.py
@@ -2,6 +2,7 @@
 import jax.numpy as jnp
 from jax import lax
 from jax.sharding import PartitionSpec as P
+from jax.lax import all_gather
 
 norm_eps = 1e-06
 
@@ -37,13 +38,18 @@
 
 
 def block_forward(values, params):
+
+    def test_positions_by_axis(x_in):
+        answer = all_gather(x_in, axis_name="tp").sum(axis=0)
+        return answer
+
     gain_vector, w_gate, w_up, w_down = params
     widened, factor, normed = normalize(values, gain_vector)
     gate_pre = jnp.dot(normed, w_gate, preferred_element_type=jnp.float32)
     up_pre = jnp.dot(normed, w_up, preferred_element_type=jnp.float32)
     hidden = (jax.nn.silu(gate_pre) * up_pre).astype(jnp.bfloat16)
-    branch = lax.psum(
-        jnp.dot(hidden, w_down, preferred_element_type=jnp.float32).astype(jnp.bfloat16), "tp"
+    branch = test_positions_by_axis(
+        jnp.dot(hidden, w_down, preferred_element_type=jnp.float32).astype(jnp.bfloat16)
     ).astype(jnp.float32)
     return (widened + 0.5 * branch).astype(jnp.bfloat16)
 

time: 562 us -> 709 us (1.26)
  waiting for transfers between devices: 447 us -> 585 us
  other arithmetic: 22 us -> 33.1 us
    all_gather x0 -> x2, waiting for transfers between devices: none -> 150 us  [test_positions_by_axis(): answer = all_gather(x_in, axis_name='tp').sum(axis=0)]
    psum x2, waiting for transfers between devices: 133 us -> 114 us  [block_backward(): lax.psum(partial_value.astype(jnp.bfloat16), 'tp').astype(jnp.float32)]
    reduce_sum x0 -> x2, other arithmetic: none -> 11.4 us  [test_positions_by_axis(): answer = all_gather(x_in, axis_name='tp').sum(axis=0)]
    all_to_all x1, waiting for transfers between devices: 8.3 us -> 18.9 us  [per_device(): lax.all_to_all(saved_first[1], 'fs', split_axis=1, concat_axis=0, tiled=T...]
  transfers between devices with their start and end apart: 9 -> 11, of which waited for: 8 -> 10; matrix products, arithmetic and copies ran while one was open for 6% -> 9% of each run, Pallas kernels for 0% -> 0%
where the time goes in v1:
time: 709 us; the launch traced here: 708 us
  waiting for transfers between devices  585 us (83%)
  matrix products  40.1 us (6%)
  other arithmetic  33.1 us (5%)
  starting transfers between devices  26.6 us (4%)
  between operations  14.4 us (2%)
  local copies, waits for them, and re-layouts  8.61 us (1%)
    all_gather x2, waiting for transfers between devices, sent_together(): whole, at, outs = (lax.all_gather(both, axis, axis=dim, tiled=True), 0, [])  166 us
    all_gather x2, waiting for transfers between devices, test_positions_by_axis(): answer = all_gather(x_in, axis_name='tp').sum(axis=0)  150 us
    psum x2, waiting for transfers between devices, block_backward(): lax.psum(partial_value.astype(jnp.bfloat16), 'tp').astype(jnp.float32)  114 us
    all_gather x1, waiting for transfers between devices, gather_turned(): whole = lax.all_gather(both, axis, axis=0, tiled=True)  72.5 us
    all_to_all x1, waiting for transfers between devices, per_device(): lax.all_to_all(saved_second[0], 'fs', split_axis=1, concat_axis=0, tiled=...  32.5 us
    all_to_all x1, waiting for transfers between devices, per_device(): lax.all_to_all(saved_first[0], 'fs', split_axis=1, concat_axis=0, tiled=T...  31.5 us
    all_to_all x1, waiting for transfers between devices, per_device(): lax.all_to_all(saved_first[1], 'fs', split_axis=1, concat_axis=0, tiled=T...  18.9 us
  transfers between devices with their start and end apart: 11, of which 10 were waited for; matrix products, arithmetic and copies ran while one was open for 9% of the time, Pallas kernels for 0%

profile of v1, /device:TPU:1, one launch (start us, length us, event | category | flops | bytes accessed | tf_op | source)
XLA Modules:
  0.0 707.5 jit_solution(12404322404854150379)
XLA Ops:
  7.2 1.5 pad_maximum_fusion.1
  8.7 0.0 all-gather.8.cloned.1.call-start
  8.8 1.6 pad_maximum_fusion
  10.4 0.0 all-reduce.3.cloned.1.call-start
  10.4 1.2 fusion.61
  11.6 1.2 fusion.53
  12.9 2.0 fusion.47
  14.9 72.5 %all-gather.10.cloned.1.call-done = bf16[2048,352]{1,0:T(8,128)(2,1)} async-done(((bf16[64,352]{1,0:T(8,128)(2,1)}), bf16[2048,352]{1,0:T(8,128)(2,1)}) %all-gather.10.cloned.1.call-update) | async-done | bytes 1441808 | tf_op jit(solution)/shard_map/all_gather | solution.py:23
  87.5 2.1 fusion.20
  89.6 70.4 %all-gather.8.cloned.1.call-done = bf16[2048,704]{1,0:T(8,128)(2,1)} async-done(((bf16[64,704]{1,0:T(8,128)(2,1)}), bf16[2048,704]{1,0:T(8,128)(2,1)}) %all-gather.8.cloned.1.call-update) | async-done | bytes 2883600 | tf_op jit(solution)/shard_map/all_gather | solution.py:12
  160.0 2.6 fusion.74
  162.6 2.6 constant_dynamic-update-slice_fusion.3
  165.3 0.7 copy-done.10
  166.0 0.7 fusion.78
  166.7 1.5 fusion
  168.2 1.6 fusion.93
  169.8 3.9 convolution_convert_fusion.1
  173.8 1.2 fusion.60
  175.0 1.2 fusion.54
  176.3 0.7 fusion.125
  177.0 0.1 copy-done.4
  177.1 1.0 fusion.85
  178.1 101.3 %all-reduce.3.cloned.1.call-done = bf16[128,2048]{1,0:T(8,128)(2,1)} async-done(((bf16[128,2048]{1,0:T(8,128)(2,1)}), bf16[128,2048]{1,0:T(8,128)(2,1)}) %all-reduce.3.cloned.1.call-update) | async-done | bytes 524304 | tf_op jit(solution)/shard_map/psum | solution.py:76
  279.4 1.7 fusion.48
  281.1 1.8 fusion.52
  282.9 0.8 copy-done.2
  283.7 0.5 convolution_multiply_fusion
  284.2 1.1 constant_dynamic-update-slice_fusion.1
  285.3 0.7 constant_dynamic-update-slice_fusion
  286.0 0.5 fusion.89
  286.5 1.5 fusion.1
  288.0 0.0 all-gather.12.cloned.1.call-start
  288.0 0.6 fusion.126
  288.7 0.2 all-gather.16.cloned.1.call-start
  288.9 81.5 %all-gather.14.cloned.1.call-done = bf16[2048,2048]{1,0:T(8,128)(2,1)} async-done(((bf16[128,2048]{1,0:T(8,128)(2,1)}), bf16[2048,2048]{1,0:T(8,128)(2,1)}) %all-gather.14.cloned.1.call-update) | async-done | bytes 8388624 | tf_op jit(solution)/shard_map/all_gather | solution.py:43
  370.4 6.1 reduce_sum.79
  376.5 1.5 fusion.65
  378.1 0.8 copy-done.6
  378.8 1.1 fusion.82
  379.9 4.0 convolution_convert_fusion
  383.9 2.1 copy.27
  386.0 13.3 %all-to-all-start = ((bf16[128,32,64]{0,2,1:T(8,128)(2,1)}), bf16[128,32,64]{0,2,1:T(8,128)(2,1)S(1)}, u32[]{:S(2)}, u32[]{:S(2)}) async-start(bf16[128,32,64]{0,2,1:T(8,128)(2,1)} %bitcast.5), calls=%async_computation | async-start | bytes 1048576 | tf_op jit(solution)/shard_map/all_to_all | solution.py:148
  399.4 2.1 copy.31
  401.4 31.5 %all-to-all-done = bf16[128,32,64]{0,2,1:T(8,128)(2,1)S(1)} async-done(((bf16[128,32,64]{0,2,1:T(8,128)(2,1)}), bf16[128,32,64]{0,2,1:T(8,128)(2,1)S(1)}, u32[]{:S(2)}, u32[]{:S(2)}) %all-to-all-start) | async-done | bytes 524320 | tf_op jit(solution)/shard_map/all_to_all | solution.py:148
  432.9 4.0 all-to-all-start.2
  436.9 1.0 copy.29
  437.9 32.5 %all-to-all-done.2 = bf16[128,32,64]{0,2,1:T(8,128)(2,1)S(1)} async-done(((bf16[128,32,64]{0,2,1:T(8,128)(2,1)}), bf16[128,32,64]{0,2,1:T(8,128)(2,1)S(1)}, u32[]{:S(2)}, u32[]{:S(2)}) %all-to-all-start.2) | async-done | bytes 524320 | tf_op jit(solution)/shard_map/all_to_all | solution.py:143
  470.5 4.5 all-to-all-start.1
  474.9 1.0 copy.33
  475.9 12.3 %all-reduce.5.cloned.1.call-done = bf16[128,2048]{1,0:T(8,128)(2,1)} async-done(((bf16[128,2048]{1,0:T(8,128)(2,1)}), bf16[128,2048]{1,0:T(8,128)(2,1)}) %all-reduce.5.cloned.1.call-update) | async-done | bytes 524304 | tf_op jit(solution)/shard_map/psum | solution.py:76
  488.2 1.4 fusion.55
  489.6 18.9 %all-to-all-done.1 = bf16[128,32,64]{0,2,1:T(8,128)(2,1)S(1)} async-done(((bf16[128,32,64]{0,2,1:T(8,128)(2,1)}), bf16[128,32,64]{0,2,1:T(8,128)(2,1)S(1)}, u32[]{:S(2)}, u32[]{:S(2)}) %all-to-all-start.1) | async-done | bytes 524320 | tf_op jit(solution)/shard_map/all_to_all | solution.py:149
  508.5 4.3 all-to-all-start.3
  512.8 2.3 fusion.59
  515.1 95.5 %all-gather.12.cloned.1.call-done = bf16[4096,1056]{0,1:T(8,128)(2,1)} async-done(((bf16[128,1056]{0,1:T(8,128)(2,1)}), bf16[4096,1056]{0,1:T(8,128)(2,1)}) %all-gather.12.cloned.1.call-update) | async-done | bytes 8650768 | tf_op jit(solution)/shard_map/all_gather | solution.py:12
  610.7 2.6 fusion.23
  613.2 2.6 fusion.26
  615.9 2.6 fusion.35
  618.4 2.6 fusion.38
  621.1 2.6 fusion.32
  623.6 2.6 fusion.44
  626.2 68.2 %all-gather.16.cloned.1.call-done = bf16[2048,2048]{1,0:T(8,128)(2,1)} async-done(((bf16[128,2048]{1,0:T(8,128)(2,1)}), bf16[2048,2048]{1,0:T(8,128)(2,1)}) %all-gather.16.cloned.1.call-update) | async-done | bytes 8388624 | tf_op jit(solution)/shard_map/all_gather | solution.py:43
  694.4 5.3 reduce_sum.81
  699.7 1.0 fusion.68
  (52 shorter events, 0.4 us)
Async XLA Ops:
  7.2 80.3 %all-gather.10.cloned.1.call-start = ((), (), s32[]{:S(2)}) async-start(), calls=%async_computation.5 | async-start | bytes 1622016 | tf_op jit(solution)/shard_map/all_gather | solution.py:23
  8.7 151.3 %all-gather.8.cloned.1.call-start = ((), (), s32[]{:S(2)}) async-start(), calls=%async_computation.4 | async-start | bytes 3244032 | tf_op jit(solution)/shard_map/all_gather | solution.py:12
  10.4 269.1 %all-reduce.3.cloned.1.call-start = ((), (), s32[]{:S(2)}) async-start(), calls=%async_computation.6 | async-start | bytes 1048576 | tf_op jit(solution)/shard_map/psum | solution.py:76
  160.0 6.0 copy-start
  165.2 3.0 copy-start.12
  165.3 0.7 copy-start.10
  168.2 202.2 %all-gather.14.cloned.1.call-start = ((), (), s32[]{:S(2)}) async-start(), calls=%async_computation.9 | async-start | bytes 8912896 | tf_op jit(solution)/shard_map/all_gather | solution.py:43
  169.8 109.6 %copy-start.11 = (f32[2048]{0:T(1024)S(1)}, f32[2048]{0:T(1024)}, u32[]{:S(2)}) copy-start(f32[2048]{0:T(1024)} %param.23) | copy-start | bytes 24580
  173.7 314.4 %all-reduce.5.cloned.1.call-start = ((), (), s32[]{:S(2)}) async-start(), calls=%async_computation.7 | async-start | bytes 1048576 | tf_op jit(solution)/shard_map/psum | solution.py:76
  176.3 0.8 copy-start.4
  279.4 4.2 copy-start.9
  279.4 4.8 copy-start.5
  282.9 0.8 copy-start.2
  288.0 322.7 %all-gather.12.cloned.1.call-start = ((), (), s32[]{:S(2)}) async-start(), calls=%async_computation.8 | async-start | bytes 8921088 | tf_op jit(solution)/shard_map/all_gather | solution.py:12
  288.7 405.8 %all-gather.16.cloned.1.call-start = ((), (), s32[]{:S(2)}) async-start(), calls=%async_computation.10 | async-start | bytes 8912896 | tf_op jit(solution)/shard_map/all_gather | solution.py:43
  378.0 0.8 copy-start.6
  383.9 53.1 %copy-start.3 = (bf16[128,2048]{1,0:T(8,128)(2,1)S(1)}, bf16[128,2048]{1,0:T(8,128)(2,1)}, u32[]{:S(2)}) copy-start(bf16[128,2048]{1,0:T(8,128)(2,1)} %copy-done.2) | copy-start | bytes 1572868
  383.9 91.0 %copy-start.8 = (bf16[128,2048]{1,0:T(8,128)(2,1)S(1)}, bf16[128,2048]{1,0:T(8,128)(2,1)}, u32[]{:S(2)}) copy-start(bf16[128,2048]{1,0:T(8,128)(2,1)} %param.21) | copy-start | bytes 1572868
  386.0 102.2 %copy-start.1 = (bf16[128,2048]{1,0:T(8,128)(2,1)S(1)}, bf16[128,2048]{1,0:T(8,128)(2,1)}, u32[]{:S(2)}) copy-start(bf16[128,2048]{1,0:T(8,128)(2,1)} %param.19) | copy-start | bytes 1572868
  386.0 46.8 %all-to-all-start = ((bf16[128,32,64]{0,2,1:T(8,128)(2,1)}), bf16[128,32,64]{0,2,1:T(8,128)(2,1)S(1)}, u32[]{:S(2)}, u32[]{:S(2)}) async-start(bf16[128,32,64]{0,2,1:T(8,128)(2,1)} %bitcast.5), calls=%async_computation | async-start | bytes 1048576 | tf_op jit(solution)/shard_map/all_to_all | solution.py:148
  432.9 37.6 %all-to-all-start.2 = ((bf16[128,32,64]{0,2,1:T(8,128)(2,1)}), bf16[128,32,64]{0,2,1:T(8,128)(2,1)S(1)}, u32[]{:S(2)}, u32[]{:S(2)}) async-start(bf16[128,32,64]{0,2,1:T(8,128)(2,1)} %bitcast.9), calls=%async_computation.2 | async-start | bytes 1048576 | tf_op jit(solution)/shard_map/all_to_all | solution.py:143
  470.5 140.2 %copy-start.13 = (f32[64,176]{1,0:T(8,128)S(1)}, f32[64,176]{1,0:T(8,128)}, u32[]{:S(2)}) copy-start(f32[64,176]{1,0:T(8,128)} %param.30) | copy-start | bytes 135172
  470.5 38.0 %all-to-all-start.1 = ((bf16[128,32,64]{0,2,1:T(8,128)(2,1)}), bf16[128,32,64]{0,2,1:T(8,128)(2,1)S(1)}, u32[]{:S(2)}, u32[]{:S(2)}) async-start(bf16[128,32,64]{0,2,1:T(8,128)(2,1)} %bitcast.7), calls=%async_computation.1 | async-start | bytes 1048576 | tf_op jit(solution)/shard_map/all_to_all | solution.py:149
  475.9 137.3 %copy-start.14 = (f32[64,176]{1,0:T(8,128)S(1)}, f32[64,176]{1,0:T(8,128)}, u32[]{:S(2)}) copy-start(f32[64,176]{1,0:T(8,128)} %param.31) | copy-start | bytes 135172
  508.5 115.2 %all-to-all-start.3 = ((bf16[128,32,64]{0,2,1:T(8,128)(2,1)}), bf16[128,32,64]{0,2,1:T(8,128)(2,1)S(1)}, u32[]{:S(2)}, u32[]{:S(2)}) async-start(bf16[128,32,64]{0,2,1:T(8,128)(2,1)} %bitcast.11), calls=%async_computation.3 | async-start | bytes 1048576 | tf_op jit(solution)/shard_map/all_to_all | solution.py:144
  512.8 103.0 %copy-start.15 = (f32[64,176]{1,0:T(8,128)S(1)}, f32[64,176]{1,0:T(8,128)}, u32[]{:S(2)}) copy-start(f32[64,176]{1,0:T(8,128)} %param.33) | copy-start | bytes 135172
  515.1 103.3 %copy-start.16 = (f32[64,176]{1,0:T(8,128)S(1)}, f32[64,176]{1,0:T(8,128)}, u32[]{:S(2)}) copy-start(f32[64,176]{1,0:T(8,128)} %param.34) | copy-start | bytes 135172
  613.2 7.8 %copy-start.17 = (f32[176,64]{0,1:T(8,128)S(1)}, f32[176,64]{0,1:T(8,128)}, u32[]{:S(2)}) copy-start(f32[176,64]{0,1:T(8,128)} %param.32) | copy-start | bytes 135172
  618.4 5.2 copy-start.18
  694.4 5.3 copy-start.7
Sparse Core Ops, SparseCore 0:
  10.7 76.7 all-gather.9
  90.1 69.8 all-gather.7
  168.3 111.0 all-reduce.2
  282.9 87.4 all-gather.13
  373.4 114.7 all-reduce.4
  490.1 120.5 all-gather.11
  614.2 80.1 all-gather.15
